TPU v7x, 32 devices: a whole 2x2x4 slice. The times are simulated.
32 devices in a mesh: kv: 8 (over z, y), tp: 4 (over x, core).
Axes of the slice: x: 2, y: 2, z: 4, core: 2. Of those that a mesh axis runs over, the one named last changes fastest.
Arguments:
- block_in: bfloat16 [64, 4096], P(None, ('kv', 'tp')), may hold values from -30 to 30
- before_gain: bfloat16 [4096], P('kv'), may hold values from 0.099609375 to 1.8984375
- before_gate: bfloat16 [4096, 11264], P('kv', 'tp'), may hold values from -0.09375 to 0.09375
- before_up: bfloat16 [4096, 11264], P('kv', 'tp'), may hold values from -0.09375 to 0.09375
- before_down: bfloat16 [11264, 4096], P('tp', 'kv'), may hold values from -0.0546875 to 0.0546875
- mix_gain: bfloat16 [4096], P('kv'), may hold values from 0.099609375 to 1.8984375
- input_gate: bfloat16 [4096, 8192], P('kv', 'tp'), may hold values from -0.09375 to 0.09375
- input_value: bfloat16 [4096, 8192], P('kv', 'tp'), may hold values from -0.09375 to 0.09375
- input_write: bfloat16 [4096, 2048], P('kv', 'tp'), may hold values from -0.09375 to 0.09375
- input_read: bfloat16 [4096, 2048], P('kv', 'tp'), may hold values from -0.09375 to 0.09375
- input_step: bfloat16 [4096, 128], P('kv', 'tp'), may hold values from -0.09375 to 0.09375
- step_bias: float32 [128], P('tp'), may hold values from -3 to 0
- decay_log: float32 [128], P('tp'), may hold values from -1 to 1.4
- skip_gain: float32 [128], P('tp'), may hold values from 0.5 to 2
- value_taps: bfloat16 [4, 8192], P(None, 'tp'), may hold values from -3 to 3
- write_taps: bfloat16 [4, 2048], P(None, 'tp'), may hold values from -3 to 3
- read_taps: bfloat16 [4, 2048], P(None, 'tp'), may hold values from -3 to 3
- value_window: bfloat16 [64, 3, 8192], P('kv', None, 'tp'), may hold values from -6 to 6
- write_window: bfloat16 [64, 3, 2048], P('kv', None, 'tp'), may hold values from -6 to 6
- read_window: bfloat16 [64, 3, 2048], P('kv', None, 'tp'), may hold values from -6 to 6
- scan_state: float32 [64, 128, 64, 128], P('kv', 'tp'), may hold values from -2 to 2
- group_gain: bfloat16 [8192], P('tp'), may hold values from 0.099609375 to 1.8984375
- mixer_out: bfloat16 [8192, 4096], P('tp', 'kv'), may hold values from -0.0625 to 0.0625
- after_gain: bfloat16 [4096], P('kv'), may hold values from 0.099609375 to 1.8984375
- after_gate: bfloat16 [4096, 11264], P('kv', 'tp'), may hold values from -0.09375 to 0.09375
- after_up: bfloat16 [4096, 11264], P('kv', 'tp'), may hold values from -0.09375 to 0.09375
- after_down: bfloat16 [11264, 4096], P('tp', 'kv'), may hold values from -0.0546875 to 0.0546875
Outputs:
- block_out: bfloat16 [64, 4096], P(None, ('kv', 'tp'))
- state_next: float32 [64, 128, 64, 128], P('kv', 'tp')
- value_next: bfloat16 [64, 3, 8192], P('kv', None, 'tp')
- write_next: bfloat16 [64, 3, 2048], P('kv', None, 'tp')
- read_next: bfloat16 [64, 3, 2048], P('kv', None, 'tp')
All inputs are finite; a program needn't handle non-finite values.
Results may differ from a plain program's by a relative error of at most 0.0085.
Values may be sent and summed in bfloat16 or wider, within the bound.
No kernel may reach another device: no remote copies, remote signals or barrier semaphores. Data moves between devices by JAX's collectives and lax.ppermute only.
A program may use at most 128 MiB of HBM per device.

v0:
```python
import jax
import jax.numpy as jnp
from jax import lax
from jax.sharding import PartitionSpec as P

D = 4096
HEAD_DIM = 64
STATE = 128


EPS = 1e-06


def lifted_rows(current, gain_vec):
    gathered = lax.all_gather(current, "tp", axis=1, tiled=True)
    widened = gathered.astype(jnp.float32)
    squares = jnp.sum(widened * widened, axis=1)
    lifted = (widened * gain_vec.astype(jnp.float32)[None, :]).astype(jnp.bfloat16)
    return (lifted, squares)


def column_sums(partial_terms):
    return lax.psum_scatter(partial_terms, "tp", scatter_dimension=1, tiled=True)


def half_channel(current, gain_vec, gate_weight, up_weight, down_weight):
    lifted, squares = lifted_rows(current, gain_vec)
    gate_part = jnp.dot(lifted, gate_weight, preferred_element_type=jnp.float32)
    up_part = jnp.dot(lifted, up_weight, preferred_element_type=jnp.float32)
    gate_sum, up_sum, totals = lax.psum((gate_part, up_part, squares), "kv")
    row_scale = lax.rsqrt(totals / D + EPS)[:, None]
    hidden = (jax.nn.silu(gate_sum * row_scale) * (up_sum * row_scale)).astype(jnp.bfloat16)
    down_sum = jnp.dot(hidden, down_weight, preferred_element_type=jnp.float32)
    returned = column_sums(down_sum)
    return (current.astype(jnp.float32) + 0.5 * returned).astype(jnp.bfloat16)


def short_conv(window_state, fresh, taps):
    window = jnp.concatenate([window_state, fresh[:, None, :]], axis=1)
    conv_sum = jnp.sum(window.astype(jnp.float32) * taps.astype(jnp.float32)[None], axis=1)
    return (jax.nn.silu(conv_sum), window[:, 1:])


def spread_groups(vectors, heads):
    count = vectors.shape[0]
    groups = vectors.shape[1] // STATE
    shaped = vectors.reshape(count, groups, 1, STATE)
    return jnp.broadcast_to(shaped, (count, groups, heads // groups, STATE)).reshape(
        count, heads, STATE
    )


def state_update(
    gate_rows,
    value_conv,
    write_conv,
    read_conv,
    step_raw,
    step_bias,
    decay_log,
    skip_gain,
    scan_state,
):
    count = value_conv.shape[0]
    heads = step_bias.shape[0]
    step_size = jax.nn.softplus(step_raw + step_bias[None, :])
    decay = jnp.exp(-step_size * jnp.exp(decay_log)[None, :])
    value_heads = value_conv.reshape(count, heads, HEAD_DIM)
    write_heads = spread_groups(write_conv, heads)
    read_heads = spread_groups(read_conv, heads)
    state_next = (
        decay[:, :, None, None] * scan_state
        + (step_size[:, :, None] * value_heads)[:, :, :, None] * write_heads[:, :, None, :]
    )
    readout = (
        jnp.sum(state_next * read_heads[:, :, None, :], axis=3)
        + skip_gain[None, :, None] * value_heads
    )
    gated = readout.reshape(count, heads * HEAD_DIM) * jax.nn.silu(gate_rows.astype(jnp.float32))
    groups = write_conv.shape[1] // STATE
    grouped = gated.reshape(count, groups, heads * HEAD_DIM // groups)
    grouped = grouped * lax.rsqrt(jnp.mean(grouped * grouped, axis=2, keepdims=True) + EPS)
    return (grouped.reshape(count, heads * HEAD_DIM), state_next)


def local(
    block_in,
    before_gain,
    before_gate,
    before_up,
    before_down,
    mix_gain,
    input_gate,
    input_value,
    input_write,
    input_read,
    input_step,
    step_bias,
    decay_log,
    skip_gain,
    value_taps,
    write_taps,
    read_taps,
    value_window,
    write_window,
    read_window,
    scan_state,
    group_gain,
    mixer_out,
    after_gain,
    after_gate,
    after_up,
    after_down,
):
    first_out = half_channel(block_in, before_gain, before_gate, before_up, before_down)
    lifted, squares = lifted_rows(first_out, mix_gain)
    gate_part = jnp.dot(lifted, input_gate, preferred_element_type=jnp.float32)
    value_part = jnp.dot(lifted, input_value, preferred_element_type=jnp.float32)
    write_part = jnp.dot(lifted, input_write, preferred_element_type=jnp.float32)
    read_part = jnp.dot(lifted, input_read, preferred_element_type=jnp.float32)
    step_part = jnp.dot(lifted, input_step, preferred_element_type=jnp.float32)
    gate_sum, value_sum, write_sum, read_sum, step_sum, totals = (
        lax.psum_scatter(gate_part, "kv", scatter_dimension=0, tiled=True),
        lax.psum_scatter(value_part, "kv", scatter_dimension=0, tiled=True),
        lax.psum_scatter(write_part, "kv", scatter_dimension=0, tiled=True),
        lax.psum_scatter(read_part, "kv", scatter_dimension=0, tiled=True),
        lax.psum_scatter(step_part, "kv", scatter_dimension=0, tiled=True),
        lax.psum_scatter(squares, "kv", scatter_dimension=0, tiled=True),
    )
    mix_scale = lax.rsqrt(totals / D + EPS)[:, None]
    gate_rows = (gate_sum * mix_scale).astype(jnp.bfloat16)
    value_fresh = (value_sum * mix_scale).astype(jnp.bfloat16)
    write_fresh = (write_sum * mix_scale).astype(jnp.bfloat16)
    read_fresh = (read_sum * mix_scale).astype(jnp.bfloat16)
    step_raw = step_sum * mix_scale
    value_conv, value_next = short_conv(value_window, value_fresh, value_taps)
    write_conv, write_next = short_conv(write_window, write_fresh, write_taps)
    read_conv, read_next = short_conv(read_window, read_fresh, read_taps)
    normed, state_next = state_update(
        gate_rows,
        value_conv,
        write_conv,
        read_conv,
        step_raw,
        step_bias,
        decay_log,
        skip_gain,
        scan_state,
    )
    mixer_rows = (normed * group_gain.astype(jnp.float32)[None, :]).astype(jnp.bfloat16)
    back_part = jnp.dot(
        lax.all_gather(mixer_rows, "kv", axis=0, tiled=True),
        mixer_out,
        preferred_element_type=jnp.float32,
    )
    returned = column_sums(back_part)
    middle = (first_out.astype(jnp.float32) + returned).astype(jnp.bfloat16)
    block_out = half_channel(middle, after_gain, after_gate, after_up, after_down)
    return (block_out, state_next, value_next, write_next, read_next)


def solution(mesh):
    placed = (
        P(None, ("kv", "tp")),
        P("kv"),
        P("kv", "tp"),
        P("kv", "tp"),
        P("tp", "kv"),
        P("kv"),
        P("kv", "tp"),
        P("kv", "tp"),
        P("kv", "tp"),
        P("kv", "tp"),
        P("kv", "tp"),
        P("tp"),
        P("tp"),
        P("tp"),
        P(None, "tp"),
        P(None, "tp"),
        P(None, "tp"),
        P("kv", None, "tp"),
        P("kv", None, "tp"),
        P("kv", None, "tp"),
        P("kv", "tp", None, None),
        P("tp"),
        P("tp", "kv"),
        P("kv"),
        P("kv", "tp"),
        P("kv", "tp"),
        P("tp", "kv"),
    )
    return jax.shard_map(
        local,
        mesh=mesh,
        in_specs=placed,
        out_specs=(
            P(None, ("kv", "tp")),
            P("kv", "tp", None, None),
            P("kv", None, "tp"),
            P("kv", None, "tp"),
            P("kv", None, "tp"),
        ),
        check_vma=False,
    )
```

profile of v0, /device:TPU:0, one launch (start us, length us, event | category | flops | bytes accessed | tf_op | source)
XLA Modules:
  0.0 575.5 jit_solution(16134604495972762844)
XLA Ops:
  7.2 0.0 all-reduce.10.cloned.1.call-start
  7.2 6.6 %all_gather.12 = bf16[64,512]{1,0:T(8,128)(2,1)S(1)} all-gather(bf16[64,128]{1,0:T(8,128)(2,1)} %param.27), channel_id=1, replica_groups=mesh['kv'=8,'tp'=4] {'tp'}, dimensions={1}, use_global_device_ids=true | all-gather | bytes 81920 | tf_op jit(solution)/shard_map/all_gather | solution.py:15
  13.8 0.7 convert_element_type.92
  14.5 1.5 fusion.21
  16.0 1.5 fusion.23
  17.5 0.0 reduce-scatter.8.cloned.1.call-start
  17.5 0.1 fusion.7
  17.6 22.7 %psum.43 = f32[64]{0:T(128)S(1)} all-reduce(f32[64]{0:T(128)S(1)} %fusion.7), channel_id=1, replica_groups=mesh['kv'=8,'tp'=4] {'kv'}, use_global_device_ids=true, to_apply=%region_2.0 | all-reduce | flops 64 | bytes 512 | tf_op jit(solution)/shard_map/psum | solution.py:30
  40.4 66.0 %all-reduce.10.cloned.1.call-done = (f32[64,2816]{1,0:T(8,128)}, f32[64,2816]{1,0:T(8,128)}) async-done(((f32[64,2816]{1,0:T(8,128)}, f32[64,2816]{1,0:T(8,128)}), (f32[64,2816]{1,0:T(8,128)}, f32[64,2816]{1,0:T(8,128)})) %all-reduce.10.cloned.1.call-update) | async-done | bytes 1441808 | tf_op jit(solution)/shard_map/psum | solution.py:30
  106.4 3.6 fusion
  110.1 0.0 reduce-scatter.12.cloned.1.call-start
  110.1 18.8 %reduce-scatter.8.cloned.1.call-done = f32[64,128]{1,0:T(8,128)} async-done(((f32[64,512]{1,0:T(8,128)}), f32[64,128]{1,0:T(8,128)}) %reduce-scatter.8.cloned.1.call-update) | async-done | bytes 32784 | tf_op jit(solution)/shard_map/reduce_scatter | solution.py:23
  129.0 0.8 add_convert_fusion.2
  129.8 5.3 all_gather.13
  135.0 0.9 fusion.30
  135.9 0.0 reduce-scatter.14.cloned.1.call-start
  135.9 1.9 fusion.28
  137.9 0.0 reduce-scatter.10.cloned.1.call-start
  137.9 2.9 fusion.32
  140.8 0.0 reduce-scatter.16.cloned.1.call-start
  140.9 0.7 exp.49
  141.6 0.7 convert_element_type.102
  142.3 0.7 mul.305
  143.0 0.7 mul.306
  143.7 0.6 convert_element_type.111
  144.3 1.2 dynamic-slice
  146.2 0.1 fusion.9
  146.3 0.9 fusion.34
  147.2 37.5 %all-reduce.2 = (f32[64]{0:T(128)S(1)}, f32[64,32]{1,0:T(8,128)S(1)}) all-reduce(f32[64]{0:T(128)S(1)} %fusion.9, f32[64,32]{1,0:T(8,128)S(1)} %fusion.34), channel_id=4, replica_groups=mesh['kv'=8,'tp'=4] {'kv'}, use_global_device_ids=true, to_apply=%region_7.8.clone | all-reduce | flops 2112 | bytes 16896
  184.7 0.1 fusion.42
  184.8 2.9 fusion.26
  187.7 0.0 reduce-scatter.18.cloned.1.call-start
  187.7 0.7 multiply_exponential_fusion
  188.4 9.5 %reduce-scatter.12.cloned.1.call-done = f32[8,512]{1,0:T(8,128)} async-done(((f32[64,512]{1,0:T(8,128)}), f32[8,512]{1,0:T(8,128)}) %reduce-scatter.12.cloned.1.call-update) | async-done | bytes 16400 | tf_op jit(solution)/shard_map/reduce_scatter | solution.py:125
  197.9 64.1 %reduce-scatter.14.cloned.1.call-done = f32[8,512]{1,0:T(8,128)} async-done(((f32[64,512]{1,0:T(8,128)}), f32[8,512]{1,0:T(8,128)}) %reduce-scatter.14.cloned.1.call-update) | async-done | bytes 16400 | tf_op jit(solution)/shard_map/reduce_scatter | solution.py:126
  262.0 0.8 fusion.38
  263.0 64.4 %reduce-scatter.10.cloned.1.call-done = f32[8,2048]{1,0:T(8,128)} async-done(((f32[64,2048]{1,0:T(8,128)}), f32[8,2048]{1,0:T(8,128)}) %reduce-scatter.10.cloned.1.call-update) | async-done | bytes 65552 | tf_op jit(solution)/shard_map/reduce_scatter | solution.py:124
  327.4 0.9 fusion.25
  328.4 0.1 reduce_sum.83
  328.5 0.8 multiply_multiply_fusion
  329.3 9.4 %multiply_reduce_fusion = (f32[8,32,64]{2,1,0:T(8,128)S(1)}, f32[8,32,64,128]{3,2,1,0:T(8,128)}) fusion(f32[8,32,128]{2,1,0:T(8,128)S(1)} %broadcast_bitcast_fusion, f32[8,32,128]{2,1,0:T(8,128)S(1)} %broadcast_bitcast_fusion.1, f32[8,32,64]{2,1,0:T(8,128)S(1)} %multiply_multiply_fusion, f32[8,32,64,128]{3,2,1,0:T(8,128)} %param.47, f32[8,32]{1,0:T(8,128)} %get-tuple-element.15), kind=kLoop, calls=%fused_computation | loop fusion | flops 10469376 | bytes 17171456 | tf_op jit(solution)/shard_map/reduce_sum | solution.py:76
  338.6 0.1 reduce_sum.89
  338.7 53.9 %reduce-scatter.16.cloned.1.call-done = f32[8,2048]{1,0:T(8,128)} async-done(((f32[64,2048]{1,0:T(8,128)}), f32[8,2048]{1,0:T(8,128)}) %reduce-scatter.16.cloned.1.call-update) | async-done | bytes 65552 | tf_op jit(solution)/shard_map/reduce_scatter | solution.py:123
  392.7 0.9 fusion.45
  393.6 0.1 reduce_sum.90
  393.7 0.1 mul.315
  393.8 0.7 multiply_convert_fusion.4
  394.5 30.9 %all_gather.14 = bf16[64,2048]{1,0:T(8,128)(2,1)S(1)} all-gather(bf16[8,2048]{1,0:T(8,128)(2,1)S(1)} %multiply_convert_fusion.4), channel_id=1, replica_groups=mesh['kv'=8,'tp'=4] {'kv'}, dimensions={0}, use_global_device_ids=true | all-gather | bytes 294912 | tf_op jit(solution)/shard_map/all_gather | solution.py:152
  425.4 2.7 fusion.47
  428.1 0.0 all-reduce.8.cloned.1.call-start
  428.2 18.7 %reduce-scatter.18.cloned.1.call-done = f32[64,128]{1,0:T(8,128)} async-done(((f32[64,512]{1,0:T(8,128)}), f32[64,128]{1,0:T(8,128)}) %reduce-scatter.18.cloned.1.call-update) | async-done | bytes 32784 | tf_op jit(solution)/shard_map/reduce_scatter | solution.py:23
  446.9 0.9 add_convert_fusion.1
  447.8 5.3 all_gather.15
  453.1 3.3 fusion.17
  456.4 1.5 fusion.19
  457.9 0.0 reduce-scatter.20.cloned.1.call-start
  457.9 0.1 fusion.11
  458.1 22.0 %psum.46 = f32[64]{0:T(128)S(1)} all-reduce(f32[64]{0:T(128)S(1)} %fusion.11), channel_id=1, replica_groups=mesh['kv'=8,'tp'=4] {'kv'}, use_global_device_ids=true, to_apply=%region_20.21 | all-reduce | flops 64 | bytes 512 | tf_op jit(solution)/shard_map/psum | solution.py:30
  480.1 65.0 %all-reduce.8.cloned.1.call-done = (f32[64,2816]{1,0:T(8,128)}, f32[64,2816]{1,0:T(8,128)}) async-done(((f32[64,2816]{1,0:T(8,128)}, f32[64,2816]{1,0:T(8,128)}), (f32[64,2816]{1,0:T(8,128)}, f32[64,2816]{1,0:T(8,128)})) %all-reduce.8.cloned.1.call-update) | async-done | bytes 1441808 | tf_op jit(solution)/shard_map/psum | solution.py:30
  545.1 3.6 fusion.1
  548.7 0.6 fusion.36
  549.3 0.7 fusion.12
  549.9 17.6 %reduce-scatter.20.cloned.1.call-done = f32[64,128]{1,0:T(8,128)} async-done(((f32[64,512]{1,0:T(8,128)}), f32[64,128]{1,0:T(8,128)}) %reduce-scatter.20.cloned.1.call-update) | async-done | bytes 32784 | tf_op jit(solution)/shard_map/reduce_scatter | solution.py:23
  567.6 1.4 add_convert_fusion
  (54 shorter events, 0.4 us)
Async XLA Ops:
  7.2 7.3 %copy-start = (bf16[512,2816]{1,0:T(8,128)(2,1)S(1)}, bf16[512,2816]{1,0:T(8,128)(2,1)}, u32[]{:S(2)}) copy-start(bf16[512,2816]{1,0:T(8,128)(2,1)} %param.30) | copy-start | bytes 8650756
  7.2 99.2 %all-reduce.10.cloned.1.call-start = ((), (), s32[]{:S(2)}) async-start(), calls=%async_computation.15 | async-start | bytes 2883584 | tf_op jit(solution)/shard_map/psum | solution.py:30
  7.2 8.7 %copy-start.1 = (bf16[512,2816]{1,0:T(8,128)(2,1)S(1)}, bf16[512,2816]{1,0:T(8,128)(2,1)}, u32[]{:S(2)}) copy-start(bf16[512,2816]{1,0:T(8,128)(2,1)} %param.29) | copy-start | bytes 8650756
  17.5 111.5 %reduce-scatter.8.cloned.1.call-start = ((), (), s32[]{:S(2)}) async-start(), calls=%async_computation.7 | async-start | bytes 163840 | tf_op jit(solution)/shard_map/reduce_scatter | solution.py:23
  106.4 3.7 copy-start.12
  106.4 22.6 %copy-start.7 = (bf16[64,128]{1,0:T(8,128)(2,1)S(1)}, bf16[64,128]{1,0:T(8,128)(2,1)}, u32[]{:S(2)}) copy-start(bf16[64,128]{1,0:T(8,128)(2,1)} %param.27) | copy-start | bytes 49156
  106.4 28.6 %copy-start.3 = (bf16[512,512]{1,0:T(8,128)(2,1)S(1)}, bf16[512,512]{1,0:T(8,128)(2,1)}, u32[]{:S(2)}) copy-start(bf16[512,512]{1,0:T(8,128)(2,1)} %param.35) | copy-start | bytes 1572868
  110.0 32.2 %copy-start.9 = (bf16[4,512]{1,0:T(4,128)(2,1)S(1)}, bf16[4,512]{1,0:T(4,128)(2,1)}, u32[]{:S(2)}) copy-start(bf16[4,512]{1,0:T(4,128)(2,1)} %param.42) | copy-start | bytes 12292
  110.0 32.2 %copy-start.10 = (bf16[4,512]{1,0:T(4,128)(2,1)S(1)}, bf16[4,512]{1,0:T(4,128)(2,1)}, u32[]{:S(2)}) copy-start(bf16[4,512]{1,0:T(4,128)(2,1)} %param.43) | copy-start | bytes 12292
  110.0 33.7 %copy-start.11 = (bf16[2048]{0:T(1024)(128)(2,1)S(1)}, bf16[2048]{0:T(1024)(128)(2,1)}, u32[]{:S(2)}) copy-start(bf16[2048]{0:T(1024)(128)(2,1)} %param.48) | copy-start | bytes 12292
  110.1 87.8 %reduce-scatter.12.cloned.1.call-start = ((), (), s32[]{:S(2)}) async-start(), calls=%async_computation.9 | async-start | bytes 147456 | tf_op jit(solution)/shard_map/reduce_scatter | solution.py:125
  135.9 126.2 %reduce-scatter.14.cloned.1.call-start = ((), (), s32[]{:S(2)}) async-start(), calls=%async_computation.10 | async-start | bytes 147456 | tf_op jit(solution)/shard_map/reduce_scatter | solution.py:126
  137.8 49.9 %copy-start.14 = (f32[32]{0:T(128)S(1)}, f32[32]{0:T(128)}, u32[]{:S(2)}) copy-start(f32[32]{0:T(128)} %param.38) | copy-start | bytes 388
  137.9 125.0 %copy-start.5 = (bf16[8,3,512]{2,0,1:T(8,128)(2,1)S(1)}, bf16[8,3,512]{2,0,1:T(8,128)(2,1)}, u32[]{:S(2)}) copy-start(bf16[8,3,512]{2,0,1:T(8,128)(2,1)} %param.46) | copy-start | bytes 73732
  137.9 125.0 %copy-start.6 = (bf16[8,3,512]{2,0,1:T(8,128)(2,1)S(1)}, bf16[8,3,512]{2,0,1:T(8,128)(2,1)}, u32[]{:S(2)}) copy-start(bf16[8,3,512]{2,0,1:T(8,128)(2,1)} %param.45) | copy-start | bytes 73732
  137.9 189.5 %reduce-scatter.10.cloned.1.call-start = ((), (), s32[]{:S(2)}) async-start(), calls=%async_computation.8 | async-start | bytes 589824 | tf_op jit(solution)/shard_map/reduce_scatter | solution.py:124
  140.8 187.5 %copy-start.4 = (bf16[8,3,2048]{2,0,1:T(8,128)(2,1)S(1)}, bf16[8,3,2048]{2,0,1:T(8,128)(2,1)}, u32[]{:S(2)}) copy-start(bf16[8,3,2048]{2,0,1:T(8,128)(2,1)} %param.44) | copy-start | bytes 294916
  140.8 251.8 %reduce-scatter.16.cloned.1.call-start = ((), (), s32[]{:S(2)}) async-start(), calls=%async_computation.11 | async-start | bytes 589824 | tf_op jit(solution)/shard_map/reduce_scatter | solution.py:123
  184.8 143.6 %copy-start.8 = (f32[8]{0:T(128)}, f32[8]{0:T(128)S(1)}, u32[]{:S(2)}) copy-start(f32[8]{0:T(128)S(1)} %fusion.42) | copy-start | bytes 100
  187.7 259.3 %reduce-scatter.18.cloned.1.call-start = ((), (), s32[]{:S(2)}) async-start(), calls=%async_computation.12 | async-start | bytes 163840 | tf_op jit(solution)/shard_map/reduce_scatter | solution.py:23
  338.6 89.6 %copy-start.13 = (bf16[512]{0:T(512)(128)(2,1)S(1)}, bf16[512]{0:T(512)(128)(2,1)}, u32[]{:S(2)}) copy-start(bf16[512]{0:T(512)(128)(2,1)} %param.50) | copy-start | bytes 3076
  428.1 116.9 %all-reduce.8.cloned.1.call-start = ((), (), s32[]{:S(2)}) async-start(), calls=%async_computation.14 | async-start | bytes 2883584 | tf_op jit(solution)/shard_map/psum | solution.py:30
  446.9 9.5 %copy-start.2 = (bf16[512,2816]{1,0:T(8,128)(2,1)S(1)}, bf16[512,2816]{1,0:T(8,128)(2,1)}, u32[]{:S(2)}) copy-start(bf16[512,2816]{1,0:T(8,128)(2,1)} %param.51) | copy-start | bytes 8650756
  457.9 109.7 %reduce-scatter.20.cloned.1.call-start = ((), (), s32[]{:S(2)}) async-start(), calls=%async_computation.13 | async-start | bytes 163840 | tf_op jit(solution)/shard_map/reduce_scatter | solution.py:23
Sparse Core Ops, SparseCore 0:
  17.6 88.7 all-reduce.9
  110.2 18.7 reduce-scatter.7
  136.0 61.8 reduce-scatter.11
  201.1 60.9 reduce-scatter.13
  265.8 61.5 reduce-scatter.9
  330.6 62.0 reduce-scatter.15
  428.3 18.6 reduce-scatter.17
  458.0 86.9 all-reduce.7
  548.8 18.7 reduce-scatter.19
where the time goes:
time: 576 us; the launch traced here: 575 us
  waiting for transfers between devices  378 us (66%)
  blocking collectives  130 us (23%)
  matrix products  27 us (5%)
  other arithmetic  21.2 us (4%)
  between operations  14.7 us (3%)
    psum x2, waiting for transfers between devices, half_channel(): gate_sum, up_sum, totals = lax.psum((gate_part, up_part, squares), 'kv')  131 us
    reduce_scatter x1, waiting for transfers between devices, local(): lax.psum_scatter(value_part, 'kv', scatter_dimension=0, tiled=True)  64.4 us
    reduce_scatter x1, waiting for transfers between devices, local(): lax.psum_scatter(read_part, 'kv', scatter_dimension=0, tiled=True)  64.1 us
    reduce_scatter x3, waiting for transfers between devices, column_sums(): lax.psum_scatter(partial_terms, 'tp', scatter_dimension=1, tiled=True)  55.2 us
    reduce_scatter x1, waiting for transfers between devices, local(): lax.psum_scatter(gate_part, 'kv', scatter_dimension=0, tiled=True)  53.9 us
    psum x2, blocking collectives, half_channel(): gate_sum, up_sum, totals = lax.psum((gate_part, up_part, squares), 'kv')  44.8 us
    unnamed x1, blocking collectives  37.5 us
    all_gather x1, blocking collectives, local(): lax.all_gather(mixer_rows, 'kv', axis=0, tiled=True)  30.9 us
  transfers between devices with their start and end apart: 9, of which 9 were waited for; matrix products, arithmetic and copies ran while one was open for 5% of the time, Pallas kernels for 0%

commit v1 on v0

--- a/solution.py
+++ b/solution.py
@@ -1,38 +1,149 @@
 import jax
 import jax.numpy as jnp
 from jax import lax
+from jax.experimental import pallas as pl
+from jax.experimental.pallas import tpu as pltpu
 from jax.sharding import PartitionSpec as P
 
 D = 4096
 HEAD_DIM = 64
 STATE = 128
+LANES = 128
 
 
 EPS = 1e-06
 
 
-def lifted_rows(current, gain_vec):
-    gathered = lax.all_gather(current, "tp", axis=1, tiled=True)
-    widened = gathered.astype(jnp.float32)
-    squares = jnp.sum(widened * widened, axis=1)
-    lifted = (widened * gain_vec.astype(jnp.float32)[None, :]).astype(jnp.bfloat16)
-    return (lifted, squares)
-
-
-def column_sums(partial_terms):
-    return lax.psum_scatter(partial_terms, "tp", scatter_dimension=1, tiled=True)
-
-
-def half_channel(current, gain_vec, gate_weight, up_weight, down_weight):
-    lifted, squares = lifted_rows(current, gain_vec)
-    gate_part = jnp.dot(lifted, gate_weight, preferred_element_type=jnp.float32)
-    up_part = jnp.dot(lifted, up_weight, preferred_element_type=jnp.float32)
-    gate_sum, up_sum, totals = lax.psum((gate_part, up_part, squares), "kv")
-    row_scale = lax.rsqrt(totals / D + EPS)[:, None]
+def exchange(blocks, axis):
+    return lax.all_to_all(blocks, axis, 0, 0)
+
+
+def spread(block, axis):
+    if axis == "tp":
+        return lax.all_gather(block, axis, axis=0)
+    return exchange(jnp.broadcast_to(block[None], (lax.axis_size(axis),) + block.shape), axis)
+
+
+def chunk_of(width):
+    count = 1
+    while width // count > 1536 and width % (LANES * (count + 1)) == 0:
+        count += 1
+    while count > 1 and width % (LANES * count):
+        count -= 1
+    return width // count
+
+
+def front(gathered, gain_vec, weights, exact_weight=None):
+    rows, depth = gathered.shape
+    exact = 0 if exact_weight is None else exact_weight.shape[1]
+    tail = LANES
+    pieces, at = [], 0
+    for index, weight in enumerate(weights):
+        size = chunk_of(weight.shape[1])
+        for start in range(0, weight.shape[1], size):
+            pieces.append((index, start, size, at))
+            at += size
+    total = at + tail
+    operands = [gathered, gain_vec.reshape(1, depth)]
+    specs = [pl.BlockSpec(memory_space=pltpu.VMEM)] * 2
+    if exact:
+        spare = jnp.zeros((depth, LANES - 2 * exact), exact_weight.dtype)
+        operands.append(jnp.concatenate([exact_weight, exact_weight, spare], axis=1))
+        specs.append(pl.BlockSpec(memory_space=pltpu.VMEM))
+    fixed = len(operands)
+
+    def kernel(*refs):
+        sources = refs[fixed : fixed + len(weights)]
+        out_ref = refs[fixed + len(weights)]
+        held = refs[fixed + len(weights) + 1 : -1]
+        arrived = refs[-1]
+        copies = []
+        for number, (index, start, size, _) in enumerate(pieces):
+            copy = pltpu.make_async_copy(
+                sources[index].at[:, pl.ds(start, size)], held[number], arrived.at[number]
+            )
+            copy.start()
+            copies.append(copy)
+        widened = refs[0][...].astype(jnp.float32)
+        lifted = (widened * refs[1][...].astype(jnp.float32)).astype(jnp.bfloat16)
+        squares = jnp.sum(widened * widened, axis=1, keepdims=True)
+        squares_high = squares.astype(jnp.bfloat16).astype(jnp.float32)
+        lane = lax.broadcasted_iota(jnp.int32, (rows, tail), 1)
+        ending = jnp.where(
+            lane == 2 * exact,
+            squares_high,
+            jnp.where(lane == 2 * exact + 1, squares - squares_high, 0.0),
+        )
+        if exact:
+            product = jnp.dot(lifted, refs[2][...], preferred_element_type=jnp.float32)
+            high = product.astype(jnp.bfloat16).astype(jnp.float32)
+            twice = jnp.where(lane < exact, high, product - high)
+            ending = jnp.where(lane < 2 * exact, twice, ending)
+        out_ref[:, pl.ds(total - tail, tail)] = ending.astype(jnp.bfloat16)
+        for number, (_, _, size, place) in enumerate(pieces):
+            copies[number].wait()
+            product = jnp.dot(lifted, held[number][...], preferred_element_type=jnp.float32)
+            out_ref[:, pl.ds(place, size)] = product.astype(jnp.bfloat16)
+
+    read = sum(weight.size for weight in weights) * 2
+    return pl.pallas_call(
+        kernel,
+        out_shape=jax.ShapeDtypeStruct((rows, total), jnp.bfloat16),
+        in_specs=specs + [pl.BlockSpec(memory_space=pl.ANY)] * len(weights),
+        out_specs=pl.BlockSpec(memory_space=pltpu.VMEM),
+        scratch_shapes=[pltpu.VMEM((depth, size), jnp.bfloat16) for _, _, size, _ in pieces]
+        + [pltpu.SemaphoreType.DMA((len(pieces),))],
+        cost_estimate=pl.CostEstimate(
+            flops=2 * rows * depth * total, bytes_accessed=read, transcendentals=0
+        ),
+        name="front",
+    )(*operands, *weights)
+
+
+def sum_over_rows_owner(sent, widths, exact):
+    devices = lax.axis_size("kv")
+    got = exchange(sent.reshape(devices, sent.shape[0] // devices, sent.shape[1]), "kv")
+    sums = jnp.sum(got.astype(jnp.float32), axis=0)
+    outs, at = [], 0
+    for width in widths:
+        outs.append(sums[:, at : at + width])
+        at += width
+    if exact:
+        outs.append(sums[:, at : at + exact] + sums[:, at + exact : at + 2 * exact])
+        at += 2 * exact
+    outs.append(sums[:, at : at + 1] + sums[:, at + 1 : at + 2])
+    return outs
+
+
+def all_rows(rows):
+    got = spread(rows, "kv")
+    return got.reshape(got.shape[0] * got.shape[1], got.shape[2])
+
+
+def tp_sum(partial):
+    return jnp.sum(spread(partial.astype(jnp.bfloat16), "tp").astype(jnp.float32), axis=0)
+
+
+def tp_column_sum(partial):
+    devices = lax.axis_size("tp")
+    rows, columns = partial.shape
+    blocks = partial.astype(jnp.bfloat16).reshape(rows, devices, columns // devices)
+    got = exchange(blocks.transpose(1, 0, 2), "tp")
+    return jnp.sum(got.astype(jnp.float32), axis=0)
+
+
+def own_columns(full):
+    size = full.shape[1] // lax.axis_size("tp")
+    return lax.dynamic_slice_in_dim(full, lax.axis_index("tp") * size, size, axis=1)
+
+
+def half_channel_part(gathered, gain_vec, gate_weight, up_weight, down_weight):
+    sent = front(gathered, gain_vec, (gate_weight, up_weight))
+    widths = (gate_weight.shape[1], up_weight.shape[1])
+    gate_sum, up_sum, totals = sum_over_rows_owner(sent, widths, 0)
+    row_scale = lax.rsqrt(totals / D + EPS)
     hidden = (jax.nn.silu(gate_sum * row_scale) * (up_sum * row_scale)).astype(jnp.bfloat16)
-    down_sum = jnp.dot(hidden, down_weight, preferred_element_type=jnp.float32)
-    returned = column_sums(down_sum)
-    return (current.astype(jnp.float32) + 0.5 * returned).astype(jnp.bfloat16)
+    return jnp.dot(all_rows(hidden), down_weight, preferred_element_type=jnp.float32)
 
 
 def short_conv(window_state, fresh, taps):
@@ -112,22 +223,16 @@
     after_up,
     after_down,
 ):
-    first_out = half_channel(block_in, before_gain, before_gate, before_up, before_down)
-    lifted, squares = lifted_rows(first_out, mix_gain)
-    gate_part = jnp.dot(lifted, input_gate, preferred_element_type=jnp.float32)
-    value_part = jnp.dot(lifted, input_value, preferred_element_type=jnp.float32)
-    write_part = jnp.dot(lifted, input_write, preferred_element_type=jnp.float32)
-    read_part = jnp.dot(lifted, input_read, preferred_element_type=jnp.float32)
-    step_part = jnp.dot(lifted, input_step, preferred_element_type=jnp.float32)
-    gate_sum, value_sum, write_sum, read_sum, step_sum, totals = (
-        lax.psum_scatter(gate_part, "kv", scatter_dimension=0, tiled=True),
-        lax.psum_scatter(value_part, "kv", scatter_dimension=0, tiled=True),
-        lax.psum_scatter(write_part, "kv", scatter_dimension=0, tiled=True),
-        lax.psum_scatter(read_part, "kv", scatter_dimension=0, tiled=True),
-        lax.psum_scatter(step_part, "kv", scatter_dimension=0, tiled=True),
-        lax.psum_scatter(squares, "kv", scatter_dimension=0, tiled=True),
-    )
-    mix_scale = lax.rsqrt(totals / D + EPS)[:, None]
+    columns = lax.all_gather(block_in, "tp", axis=1, tiled=True)
+    down_part = half_channel_part(columns, before_gain, before_gate, before_up, before_down)
+    first_out = (columns.astype(jnp.float32) + 0.5 * tp_sum(down_part)).astype(jnp.bfloat16)
+    mixed = (input_gate, input_value, input_write, input_read)
+    sent = front(first_out, mix_gain, mixed, input_step)
+    widths = tuple(weight.shape[1] for weight in mixed)
+    gate_sum, value_sum, write_sum, read_sum, step_sum, totals = sum_over_rows_owner(
+        sent, widths, input_step.shape[1]
+    )
+    mix_scale = lax.rsqrt(totals / D + EPS)
     gate_rows = (gate_sum * mix_scale).astype(jnp.bfloat16)
     value_fresh = (value_sum * mix_scale).astype(jnp.bfloat16)
     write_fresh = (write_sum * mix_scale).astype(jnp.bfloat16)
@@ -148,14 +253,11 @@
         scan_state,
     )
     mixer_rows = (normed * group_gain.astype(jnp.float32)[None, :]).astype(jnp.bfloat16)
-    back_part = jnp.dot(
-        lax.all_gather(mixer_rows, "kv", axis=0, tiled=True),
-        mixer_out,
-        preferred_element_type=jnp.float32,
-    )
-    returned = column_sums(back_part)
-    middle = (first_out.astype(jnp.float32) + returned).astype(jnp.bfloat16)
-    block_out = half_channel(middle, after_gain, after_gate, after_up, after_down)
+    back_part = jnp.dot(all_rows(mixer_rows), mixer_out, preferred_element_type=jnp.float32)
+    middle = (first_out.astype(jnp.float32) + tp_sum(back_part)).astype(jnp.bfloat16)
+    down_part = half_channel_part(middle, after_gain, after_gate, after_up, after_down)
+    returned = tp_column_sum(down_part)
+    block_out = (own_columns(middle).astype(jnp.float32) + 0.5 * returned).astype(jnp.bfloat16)
     return (block_out, state_next, value_next, write_next, read_next)
 
 

time: 576 us -> 184 us (0.32)
  waiting for transfers between devices: 378 us -> 41.2 us
  blocking collectives: 130 us -> 68.8 us
  matrix products: 27 us -> 5.09 us
  starting transfers between devices: 0.37 us -> 17.8 us
  Pallas kernels: 0 us -> 14.3 us
  between operations: 14.7 us -> 0.92 us
  local copies, waits for them, and re-layouts: 3.67 us -> 10.1 us
    reduce_scatter x7 -> x0, waiting for transfers between devices: 247 us -> none  [the longest x1 64.4 us: local(): lax.psum_scatter(value_part, 'kv', scatter_dimension=0, tiled=True)]
    psum x2 -> x0, waiting for transfers between devices: 131 us -> none  [half_channel(): gate_sum, up_sum, totals = lax.psum((gate_part, up_part, squares), 'kv')]
    all_to_all x0 -> x2, blocking collectives: none -> 48.9 us  [exchange(): return lax.all_to_all(blocks, axis, 0, 0)]
    psum x2 -> x0, blocking collectives: 44.8 us -> none  [half_channel(): gate_sum, up_sum, totals = lax.psum((gate_part, up_part, squares), 'kv')]
    all_to_all x0 -> x5, waiting for transfers between devices: none -> 41.2 us  [exchange(): return lax.all_to_all(blocks, axis, 0, 0)]
    unnamed x1 -> x0, blocking collectives: 37.5 us -> none
    all_gather x4 -> x3, blocking collectives: 48 us -> 19.9 us  [the longest x2 11.6 us: spread(): return lax.all_gather(block, axis, axis=0)]
    dot_general x12 -> x3, matrix products: 27 us -> 5.09 us  [the longest x2 3.03 us: half_channel_part(): jnp.dot(all_rows(hidden), down_weight, preferred_element_type=jnp.float32)]
  transfers between devices with their start and end apart: 9 -> 5, of which waited for: 9 -> 5; matrix products, arithmetic and copies ran while one was open for 5% -> 7% of each run, Pallas kernels for 0% -> 0%
where the time goes in v1:
time: 184 us; the launch traced here: 183 us
  blocking collectives  68.8 us (37%)
  waiting for transfers between devices  41.2 us (22%)
  other arithmetic  24.3 us (13%)
  starting transfers between devices  17.8 us (10%)
  Pallas kernels  14.3 us (8%)
  local copies, waits for them, and re-layouts  10.1 us (5%)
  matrix products  5.09 us (3%)
    all_to_all x2, blocking collectives, exchange(): return lax.all_to_all(blocks, axis, 0, 0)  48.9 us
    all_to_all x5, waiting for transfers between devices, exchange(): return lax.all_to_all(blocks, axis, 0, 0)  41.2 us
    all_to_all x5, starting transfers between devices, exchange(): return lax.all_to_all(blocks, axis, 0, 0)  17.8 us
    pallas_call x3, Pallas kernels, front(): pl.pallas_call(kernel, out_shape=jax.ShapeDtypeStruct((rows, total), jnp....  14.3 us
    all_gather x2, blocking collectives, spread(): return lax.all_gather(block, axis, axis=0)  11.6 us
    reduce_sum x1, other arithmetic, state_update(): jnp.sum(state_next * read_heads[:, :, None, :], axis=3)  9.36 us
    all_gather x1, blocking collectives, local(): columns = lax.all_gather(block_in, 'tp', axis=1, tiled=True)  8.38 us
    convert_element_type x3, other arithmetic, short_conv(): taps.astype(jnp.float32)[None]  3.91 us
  transfers between devices with their start and end apart: 5, of which 5 were waited for; matrix products, arithmetic and copies ran while one was open for 7% of the time, Pallas kernels for 0%

profile of v1, /device:TPU:0, one launch (start us, length us, event | category | flops | bytes accessed | tf_op | source)
XLA Modules:
  0.0 182.5 jit_solution(3003717300620068664)
XLA Ops:
  0.6 8.4 %all_gather.15.refs_0_ = bf16[64,512]{1,0:T(8,128)(2,1)} all-gather(bf16[64,128]{1,0:T(8,128)(2,1)} %param.27), channel_id=1, replica_groups=mesh['kv'=8,'tp'=4] {'tp'}, dimensions={1}, use_global_device_ids=true | all-gather | bytes 81920 | tf_op jit(solution)/shard_map/all_gather | solution.py:226
  9.0 1.3 reshape.110.refs_1_
  10.3 4.8 %front.3 = bf16[64,5760]{1,0:T(8,128)(2,1)} custom-call(bf16[64,512]{1,0:T(8,128)(2,1)} %all_gather.15.refs_0_, bf16[1,512]{1,0:T(2,128)(2,1)} %reshape.110.refs_1_, bf16[512,2816]{1,0:T(8,128)(2,1)} %refs_2_.2, bf16[512,2816]{1,0:T(8,128)(2,1)} %refs_3_.3), custom_call_target="tpu_custom_call" | custom-call | flops 377487360 | bytes 5767168 | tf_op jit(solution)/shard_map/front/pallas_call | solution.py:89
  15.1 25.4 %all_to_all.35 = bf16[8,8,5760]{2,1,0:T(8,128)(2,1)S(1)} all-to-all(bf16[8,8,5760]{2,1,0:T(8,128)(2,1)} %bitcast.39), channel_id=1, replica_groups=mesh['kv'=8,'tp'=4] {'kv'}, dimensions={0} | all-to-all | bytes 1474560 | tf_op jit(solution)/shard_map/all_to_all | solution.py:18
  40.6 0.1 convert_reduce_fusion.1
  40.7 0.2 fusion.35
  40.8 0.1 fusion.8
  41.0 0.8 broadcast_in_dim.18
  41.7 3.6 %all-to-all-start.1 = ((bf16[8,8,2816]{2,1,0:T(8,128)(2,1)}), bf16[8,8,2816]{2,1,0:T(8,128)(2,1)S(1)}, u32[]{:S(2)}, u32[]{:S(2)}) async-start(bf16[8,8,2816]{2,1,0:T(8,128)(2,1)} %broadcast_in_dim.18), calls=%async_computation.1 | async-start | bytes 720896 | tf_op jit(solution)/shard_map/all_to_all | solution.py:18
  45.3 0.1 copy.36
  45.5 0.6 reshape.113.refs_1_
  46.0 0.1 pad.8.clone
  46.1 0.7 maximum_maximum_fusion.refs_2_
  46.9 9.5 %all-to-all-done.1 = bf16[8,8,2816]{2,1,0:T(8,128)(2,1)S(1)} async-done(((bf16[8,8,2816]{2,1,0:T(8,128)(2,1)}), bf16[8,8,2816]{2,1,0:T(8,128)(2,1)S(1)}, u32[]{:S(2)}, u32[]{:S(2)}) %all-to-all-start.1) | async-done | bytes 360480 | tf_op jit(solution)/shard_map/all_to_all | solution.py:18
  56.4 0.6 convolution_convert_fusion.1
  57.0 5.8 %all-gather = bf16[256,512]{1,0:T(8,128)(2,1)S(1)} all-gather(bf16[64,512]{1,0:T(8,128)(2,1)S(1)} %convolution_convert_fusion.1), channel_id=2, replica_groups=mesh['kv'=8,'tp'=4] {'tp'}, dimensions={0}, use_global_device_ids=true | all-gather | bytes 327680 | tf_op jit(solution)/shard_map/all_gather | solution.py:23
  62.8 0.7 add_convert_fusion.1.refs_0_
  63.5 4.7 %front.4 = bf16[64,5248]{1,0:T(8,128)(2,1)} custom-call(bf16[64,512]{1,0:T(8,128)(2,1)} %add_convert_fusion.1.refs_0_, bf16[1,512]{1,0:T(2,128)(2,1)} %reshape.113.refs_1_, bf16[512,128]{1,0:T(8,128)(2,1)} %maximum_maximum_fusion.refs_2_, bf16[512,2048]{1,0:T(8,128)(2,1)} %refs_3_.4, bf16[512,2048]{1,0:T(8,128)(2,1)} %refs_4_.1, bf16[512,512]{1,0:T(8,128)(2,1)} %refs_5_.1, ...), custom_call_target="tpu_custom_call" | custom-call | flops 343932928 | bytes 5242880 | tf_op jit(solution)/shard_map/front/pallas_call | solution.py:89
  68.2 3.6 %all-to-all-start.2 = ((bf16[8,8,5248]{2,1,0:T(8,128)(2,1)}), bf16[8,8,5248]{2,1,0:T(8,128)(2,1)S(1)}, u32[]{:S(2)}, u32[]{:S(2)}) async-start(bf16[8,8,5248]{2,1,0:T(8,128)(2,1)} %bitcast.41), calls=%async_computation.2 | async-start | bytes 1343488 | tf_op jit(solution)/shard_map/all_to_all | solution.py:18
  71.9 1.3 convert_element_type.103
  73.1 1.3 convert_element_type.106
  74.4 1.3 convert_element_type.100
  75.8 1.2 exp.49
  76.9 1.3 mul.284
  78.3 1.4 mul.285
  79.7 1.3 convert_element_type.109
  80.9 9.2 %all-to-all-done.2 = bf16[8,8,5248]{2,1,0:T(8,128)(2,1)S(1)} async-done(((bf16[8,8,5248]{2,1,0:T(8,128)(2,1)}), bf16[8,8,5248]{2,1,0:T(8,128)(2,1)S(1)}, u32[]{:S(2)}, u32[]{:S(2)}) %all-to-all-start.2) | async-done | bytes 671776 | tf_op jit(solution)/shard_map/all_to_all | solution.py:18
  90.2 0.1 convert_reduce_fusion.2
  90.3 0.2 fusion.29
  90.5 0.1 fusion.20
  90.5 0.4 copy-done.1
  90.9 0.1 fusion.15
  91.0 0.8 multiply_reduce_fusion.2
  91.9 0.9 multiply_reduce_fusion.1
  92.9 0.1 reduce_sum.111
  92.9 0.8 multiply_exponential_fusion
  93.8 0.1 multiply_multiply_fusion
  93.9 9.4 %multiply_reduce_fusion = (f32[8,32,64]{2,1,0:T(8,128)S(1)}, f32[8,32,64,128]{3,2,1,0:T(8,128)}) fusion(f32[8,32,128]{2,1,0:T(8,128)S(1)} %broadcast_bitcast_fusion, f32[8,32,128]{2,1,0:T(8,128)S(1)} %broadcast_bitcast_fusion.1, f32[8,32,64]{2,1,0:T(8,128)S(1)} %multiply_multiply_fusion, f32[8,32,64,128]{3,2,1,0:T(8,128)} %param.47, ...), kind=kLoop, calls=%fused_computation | loop fusion | flops 10469376 | bytes 17171456 | tf_op jit(solution)/shard_map/reduce_sum | solution.py:187
  103.3 0.1 reduce_sum.117
  103.4 0.9 fusion.36
  104.3 0.1 reduce_sum.118
  104.4 0.1 mul.294
  104.5 0.7 broadcast_in_dim.25
  105.3 3.6 %all-to-all-start.3 = ((bf16[8,8,2048]{2,1,0:T(8,128)(2,1)}), bf16[8,8,2048]{2,1,0:T(8,128)(2,1)S(1)}, u32[]{:S(2)}, u32[]{:S(2)}) async-start(bf16[8,8,2048]{2,1,0:T(8,128)(2,1)} %broadcast_in_dim.25), calls=%async_computation.3 | async-start | bytes 524288 | tf_op jit(solution)/shard_map/all_to_all | solution.py:18
  108.9 0.6 reshape.116.refs_1_
  109.5 8.5 %all-to-all-done.3 = bf16[8,8,2048]{2,1,0:T(8,128)(2,1)S(1)} async-done(((bf16[8,8,2048]{2,1,0:T(8,128)(2,1)}), bf16[8,8,2048]{2,1,0:T(8,128)(2,1)S(1)}, u32[]{:S(2)}, u32[]{:S(2)}) %all-to-all-start.3) | async-done | bytes 262176 | tf_op jit(solution)/shard_map/all_to_all | solution.py:18
  118.0 2.1 %convolution_convert_fusion.2 = bf16[64,512]{1,0:T(8,128)(2,1)S(1)} fusion(bf16[2048,512]{1,0:T(8,128)(2,1)} %param.49, bf16[8,8,2048]{2,1,0:T(8,128)(2,1)S(1)} %all-to-all-done.3), kind=kOutput, calls=%fused_computation.7 | convolution fusion | flops 134250496 | bytes 2424832 | tf_op jit(solution)/shard_map/dot_general | solution.py:256
  120.1 5.8 %all-gather.1 = bf16[256,512]{1,0:T(8,128)(2,1)S(1)} all-gather(bf16[64,512]{1,0:T(8,128)(2,1)S(1)} %convolution_convert_fusion.2), channel_id=3, replica_groups=mesh['kv'=8,'tp'=4] {'tp'}, dimensions={0}, use_global_device_ids=true | all-gather | bytes 327680 | tf_op jit(solution)/shard_map/all_gather | solution.py:23
  125.9 0.6 add_convert_fusion.refs_0_
  126.5 4.8 %front.5 = bf16[64,5760]{1,0:T(8,128)(2,1)} custom-call(bf16[64,512]{1,0:T(8,128)(2,1)} %add_convert_fusion.refs_0_, bf16[1,512]{1,0:T(2,128)(2,1)} %reshape.116.refs_1_, bf16[512,2816]{1,0:T(8,128)(2,1)} %refs_2_.3, bf16[512,2816]{1,0:T(8,128)(2,1)} %refs_3_.5), custom_call_target="tpu_custom_call" | custom-call | flops 377487360 | bytes 5767168 | tf_op jit(solution)/shard_map/front/pallas_call | solution.py:89
  131.4 23.4 %all_to_all.36 = bf16[8,8,5760]{2,1,0:T(8,128)(2,1)S(1)} all-to-all(bf16[8,8,5760]{2,1,0:T(8,128)(2,1)} %bitcast.40), channel_id=1, replica_groups=mesh['kv'=8,'tp'=4] {'kv'}, dimensions={0} | all-to-all | bytes 1474560 | tf_op jit(solution)/shard_map/all_to_all | solution.py:18
  154.8 0.1 convert_reduce_fusion
  154.9 0.2 fusion.25
  155.1 0.1 fusion.6
  155.2 0.8 broadcast_in_dim.26
  155.9 3.6 %all-to-all-start.5 = ((bf16[8,8,2816]{2,1,0:T(8,128)(2,1)}), bf16[8,8,2816]{2,1,0:T(8,128)(2,1)S(1)}, u32[]{:S(2)}, u32[]{:S(2)}) async-start(bf16[8,8,2816]{2,1,0:T(8,128)(2,1)} %broadcast_in_dim.26), calls=%async_computation.5 | async-start | bytes 720896 | tf_op jit(solution)/shard_map/all_to_all | solution.py:18
  159.6 0.7 fusion.4
  160.2 10.5 %all-to-all-done.5 = bf16[8,8,2816]{2,1,0:T(8,128)(2,1)S(1)} async-done(((bf16[8,8,2816]{2,1,0:T(8,128)(2,1)}), bf16[8,8,2816]{2,1,0:T(8,128)(2,1)S(1)}, u32[]{:S(2)}, u32[]{:S(2)}) %all-to-all-start.5) | async-done | bytes 360480 | tf_op jit(solution)/shard_map/all_to_all | solution.py:18
  170.8 2.4 %fusion = bf16[8,4,8,128]{3,2,1,0:T(8,128)(2,1)S(1)} fusion(bf16[2816,512]{1,0:T(8,128)(2,1)} %param.53, bf16[8,8,2816]{2,1,0:T(8,128)(2,1)S(1)} %all-to-all-done.5), kind=kOutput, calls=%fused_computation.8 | convolution fusion | flops 184582144 | bytes 3309568 | tf_op jit(solution)/shard_map/dot_general | solution.py:146
  173.2 0.6 copy.41
  173.8 3.3 %all-to-all-start.6 = ((bf16[4,64,128]{2,1,0:T(8,128)(2,1)}), bf16[4,64,128]{2,1,0:T(8,128)(2,1)S(1)}, u32[]{:S(2)}, u32[]{:S(2)}) async-start(bf16[4,64,128]{2,1,0:T(8,128)(2,1)} %bitcast.38), calls=%async_computation.6 | async-start | bytes 131072 | tf_op jit(solution)/shard_map/all_to_all | solution.py:18
  177.1 0.6 fusion.16
  177.7 3.4 %all-to-all-done.6 = bf16[4,64,128]{2,1,0:T(8,128)(2,1)S(1)} async-done(((bf16[4,64,128]{2,1,0:T(8,128)(2,1)}), bf16[4,64,128]{2,1,0:T(8,128)(2,1)S(1)}, u32[]{:S(2)}, u32[]{:S(2)}) %all-to-all-start.6) | async-done | bytes 65568 | tf_op jit(solution)/shard_map/all_to_all | solution.py:18
  181.2 1.3 add_convert_fusion.2
  (35 shorter events, 0.3 us)
Async XLA Ops:
  0.6 55.7 %copy-start = (bf16[2816,512]{1,0:T(8,128)(2,1)S(1)}, bf16[2816,512]{1,0:T(8,128)(2,1)}, u32[]{:S(2)}) copy-start(bf16[2816,512]{1,0:T(8,128)(2,1)} %param.31) | copy-start | bytes 8650756
  15.1 30.2 %copy-start.7 = (bf16[512,32]{0,1:T(8,128)(2,1)S(1)}, bf16[512,32]{0,1:T(8,128)(2,1)}, u32[]{:S(2)}) copy-start(bf16[512,32]{0,1:T(8,128)(2,1)} %param.37) | copy-start | bytes 98308
  15.1 30.3 %copy-start.10 = (bf16[512]{0:T(512)(128)(2,1)S(1)}, bf16[512]{0:T(512)(128)(2,1)}, u32[]{:S(2)}) copy-start(bf16[512]{0:T(512)(128)(2,1)} %param.32) | copy-start | bytes 3076
  40.8 22.0 %copy-start.2 = (bf16[64,512]{1,0:T(8,128)(2,1)S(1)}, bf16[64,512]{1,0:T(8,128)(2,1)}, u32[]{:S(2)}) copy-start(bf16[64,512]{1,0:T(8,128)(2,1)} %all_gather.15.refs_0_) | copy-start | bytes 196612
  41.7 14.6 %all-to-all-start.1 = ((bf16[8,8,2816]{2,1,0:T(8,128)(2,1)}), bf16[8,8,2816]{2,1,0:T(8,128)(2,1)S(1)}, u32[]{:S(2)}, u32[]{:S(2)}) async-start(bf16[8,8,2816]{2,1,0:T(8,128)(2,1)} %broadcast_in_dim.18), calls=%async_computation.1 | async-start | bytes 720896 | tf_op jit(solution)/shard_map/all_to_all | solution.py:18
  68.2 22.0 %all-to-all-start.2 = ((bf16[8,8,5248]{2,1,0:T(8,128)(2,1)}), bf16[8,8,5248]{2,1,0:T(8,128)(2,1)S(1)}, u32[]{:S(2)}, u32[]{:S(2)}) async-start(bf16[8,8,5248]{2,1,0:T(8,128)(2,1)} %bitcast.41), calls=%async_computation.2 | async-start | bytes 1343488 | tf_op jit(solution)/shard_map/all_to_all | solution.py:18
  90.3 0.7 copy-start.1
  93.9 9.5 %copy-start.9 = (f32[2048]{0:T(1024)S(1)}, f32[2048]{0:T(1024)}, u32[]{:S(2)}) copy-start(f32[2048]{0:T(1024)} %mul.285) | copy-start | bytes 24580
  93.9 10.6 %copy-start.8 = (f32[2048]{0:T(1024)S(1)}, f32[2048]{0:T(1024)}, u32[]{:S(2)}) copy-start(f32[2048]{0:T(1024)} %convert_element_type.109) | copy-start | bytes 24580
  93.9 15.0 %copy-start.11 = (bf16[512]{0:T(512)(128)(2,1)S(1)}, bf16[512]{0:T(512)(128)(2,1)}, u32[]{:S(2)}) copy-start(bf16[512]{0:T(512)(128)(2,1)} %param.50) | copy-start | bytes 3076
  103.3 22.6 %copy-start.3 = (bf16[64,512]{1,0:T(8,128)(2,1)S(1)}, bf16[64,512]{1,0:T(8,128)(2,1)}, u32[]{:S(2)}) copy-start(bf16[64,512]{1,0:T(8,128)(2,1)} %add_convert_fusion.1.refs_0_) | copy-start | bytes 196612
  105.3 12.7 %all-to-all-start.3 = ((bf16[8,8,2048]{2,1,0:T(8,128)(2,1)}), bf16[8,8,2048]{2,1,0:T(8,128)(2,1)S(1)}, u32[]{:S(2)}, u32[]{:S(2)}) async-start(bf16[8,8,2048]{2,1,0:T(8,128)(2,1)} %broadcast_in_dim.25), calls=%async_computation.3 | async-start | bytes 524288 | tf_op jit(solution)/shard_map/all_to_all | solution.py:18
  131.3 28.2 %copy-start.4 = (bf16[8,3,2048]{2,0,1:T(8,128)(2,1)S(1)}, bf16[8,3,2048]{2,0,1:T(8,128)(2,1)}, u32[]{:S(2)}) copy-start(bf16[8,3,2048]{2,0,1:T(8,128)(2,1)} %param.44) | copy-start | bytes 294916
  154.8 22.3 %copy-start.5 = (bf16[8,3,512]{2,0,1:T(8,128)(2,1)S(1)}, bf16[8,3,512]{2,0,1:T(8,128)(2,1)}, u32[]{:S(2)}) copy-start(bf16[8,3,512]{2,0,1:T(8,128)(2,1)} %param.46) | copy-start | bytes 73732
  154.8 22.3 %copy-start.6 = (bf16[8,3,512]{2,0,1:T(8,128)(2,1)S(1)}, bf16[8,3,512]{2,0,1:T(8,128)(2,1)}, u32[]{:S(2)}) copy-start(bf16[8,3,512]{2,0,1:T(8,128)(2,1)} %param.45) | copy-start | bytes 73732
  155.9 14.8 %all-to-all-start.5 = ((bf16[8,8,2816]{2,1,0:T(8,128)(2,1)}), bf16[8,8,2816]{2,1,0:T(8,128)(2,1)S(1)}, u32[]{:S(2)}, u32[]{:S(2)}) async-start(bf16[8,8,2816]{2,1,0:T(8,128)(2,1)} %broadcast_in_dim.26), calls=%async_computation.5 | async-start | bytes 720896 | tf_op jit(solution)/shard_map/all_to_all | solution.py:18
  173.8 7.4 %all-to-all-start.6 = ((bf16[4,64,128]{2,1,0:T(8,128)(2,1)}), bf16[4,64,128]{2,1,0:T(8,128)(2,1)S(1)}, u32[]{:S(2)}, u32[]{:S(2)}) async-start(bf16[4,64,128]{2,1,0:T(8,128)(2,1)} %bitcast.38), calls=%async_computation.6 | async-start | bytes 131072 | tf_op jit(solution)/shard_map/all_to_all | solution.py:18

commit v2 on v1

--- a/solution.py
+++ b/solution.py
@@ -25,12 +25,9 @@
 
 
 def chunk_of(width):
-    count = 1
-    while width // count > 1536 and width % (LANES * (count + 1)) == 0:
-        count += 1
-    while count > 1 and width % (LANES * count):
-        count -= 1
-    return width // count
+    lanes = width // LANES
+    fits = [n for n in range(1, lanes + 1) if lanes % n == 0 and n * LANES <= 4096]
+    return max(fits) * LANES if width % LANES == 0 else width
 
 
 def front(gathered, gain_vec, weights, exact_weight=None):
@@ -44,7 +41,7 @@
             pieces.append((index, start, size, at))
             at += size
     total = at + tail
-    operands = [gathered, gain_vec.reshape(1, depth)]
+    operands = [gathered, gain_vec]
     specs = [pl.BlockSpec(memory_space=pltpu.VMEM)] * 2
     if exact:
         spare = jnp.zeros((depth, LANES - 2 * exact), exact_weight.dtype)
@@ -55,17 +52,8 @@
     def kernel(*refs):
         sources = refs[fixed : fixed + len(weights)]
         out_ref = refs[fixed + len(weights)]
-        held = refs[fixed + len(weights) + 1 : -1]
-        arrived = refs[-1]
-        copies = []
-        for number, (index, start, size, _) in enumerate(pieces):
-            copy = pltpu.make_async_copy(
-                sources[index].at[:, pl.ds(start, size)], held[number], arrived.at[number]
-            )
-            copy.start()
-            copies.append(copy)
         widened = refs[0][...].astype(jnp.float32)
-        lifted = (widened * refs[1][...].astype(jnp.float32)).astype(jnp.bfloat16)
+        lifted = (widened * refs[1][...].astype(jnp.float32)[None, :]).astype(jnp.bfloat16)
         squares = jnp.sum(widened * widened, axis=1, keepdims=True)
         squares_high = squares.astype(jnp.bfloat16).astype(jnp.float32)
         lane = lax.broadcasted_iota(jnp.int32, (rows, tail), 1)
@@ -80,19 +68,18 @@
             twice = jnp.where(lane < exact, high, product - high)
             ending = jnp.where(lane < 2 * exact, twice, ending)
         out_ref[:, pl.ds(total - tail, tail)] = ending.astype(jnp.bfloat16)
-        for number, (_, _, size, place) in enumerate(pieces):
-            copies[number].wait()
-            product = jnp.dot(lifted, held[number][...], preferred_element_type=jnp.float32)
+        for index, start, size, place in pieces:
+            weight = sources[index][:, pl.ds(start, size)]
+            product = jnp.dot(lifted, weight, preferred_element_type=jnp.float32)
             out_ref[:, pl.ds(place, size)] = product.astype(jnp.bfloat16)
 
     read = sum(weight.size for weight in weights) * 2
     return pl.pallas_call(
         kernel,
         out_shape=jax.ShapeDtypeStruct((rows, total), jnp.bfloat16),
-        in_specs=specs + [pl.BlockSpec(memory_space=pl.ANY)] * len(weights),
+        in_specs=specs + [pl.BlockSpec(memory_space=pltpu.VMEM)] * len(weights),
         out_specs=pl.BlockSpec(memory_space=pltpu.VMEM),
-        scratch_shapes=[pltpu.VMEM((depth, size), jnp.bfloat16) for _, _, size, _ in pieces]
-        + [pltpu.SemaphoreType.DMA((len(pieces),))],
+        compiler_params=pltpu.CompilerParams(vmem_limit_bytes=16 << 20),
         cost_estimate=pl.CostEstimate(
             flops=2 * rows * depth * total, bytes_accessed=read, transcendentals=0
         ),

time: 184 us -> 181 us (0.984)
  blocking collectives: 68.8 us -> 79.4 us
  Pallas kernels: 14.3 us -> 4.12 us
  local copies, waits for them, and re-layouts: 10.1 us -> 15.6 us
  waiting for transfers between devices: 41.2 us -> 35.9 us
  starting transfers between devices: 17.8 us -> 15.3 us
  other arithmetic: 24.3 us -> 22 us
    all_to_all x2 -> x3, blocking collectives: 48.9 us -> 61.3 us  [exchange(): return lax.all_to_all(blocks, axis, 0, 0)]
    pallas_call x3, Pallas kernels: 14.3 us -> 4.12 us  [front(): pl.pallas_call(kernel, out_shape=jax.ShapeDtypeStruct((rows, total), jnp....]
    unnamed x25 -> x53, local copies, waits for them, and re-layouts: 0.57 us -> 8.91 us
    all_to_all x5 -> x4, waiting for transfers between devices: 41.2 us -> 35.9 us  [exchange(): return lax.all_to_all(blocks, axis, 0, 0)]
    convert_element_type x3, other arithmetic: 3.91 us -> 0.62 us  [short_conv(): taps.astype(jnp.float32)[None]]
    all_to_all x5 -> x4, starting transfers between devices: 17.8 us -> 15.3 us  [exchange(): return lax.all_to_all(blocks, axis, 0, 0)]
    reshape x3 -> x0, local copies, waits for them, and re-layouts: 2.42 us -> none  [front(): operands = [gathered, gain_vec.reshape(1, depth)]]
  transfers between devices with their start and end apart: 5 -> 4, of which waited for: 5 -> 4; matrix products, arithmetic and copies ran while one was open for 7% -> 5% of each run, Pallas kernels for 0% -> 0%
where the time goes in v2:
time: 181 us; the launch traced here: 180 us
  blocking collectives  79.4 us (44%)
  waiting for transfers between devices  35.9 us (20%)
  other arithmetic  22 us (12%)
  local copies, waits for them, and re-layouts  15.6 us (9%)
  starting transfers between devices  15.3 us (8%)
  matrix products  6.22 us (3%)
  Pallas kernels  4.12 us (2%)
    all_to_all x3, blocking collectives, exchange(): return lax.all_to_all(blocks, axis, 0, 0)  61.3 us
    all_to_all x4, waiting for transfers between devices, exchange(): return lax.all_to_all(blocks, axis, 0, 0)  35.9 us
    all_to_all x4, starting transfers between devices, exchange(): return lax.all_to_all(blocks, axis, 0, 0)  15.3 us
    all_gather x2, blocking collectives, spread(): return lax.all_gather(block, axis, axis=0)  11.6 us
    reduce_sum x1, other arithmetic, state_update(): jnp.sum(state_next * read_heads[:, :, None, :], axis=3)  8.98 us
    unnamed x53, local copies, waits for them, and re-layouts  8.91 us
    all_gather x1, blocking collectives, local(): columns = lax.all_gather(block_in, 'tp', axis=1, tiled=True)  6.58 us
    dot_general x2, matrix products, half_channel_part(): jnp.dot(all_rows(hidden), down_weight, preferred_element_type=jnp.float32)  4.16 us
  transfers between devices with their start and end apart: 4, of which 4 were waited for; matrix products, arithmetic and copies ran while one was open for 5% of the time, Pallas kernels for 0%

profile of v2, /device:TPU:0, one launch (start us, length us, event | category | flops | bytes accessed | tf_op | source)
XLA Modules:
  0.0 179.5 jit_solution(1818114946601316034)
XLA Ops:
  0.6 0.0 copy-start
  0.6 6.6 %all_gather.15.refs_0_ = bf16[64,512]{1,0:T(8,128)(2,1)S(1)} all-gather(bf16[64,128]{1,0:T(8,128)(2,1)} %param.27), channel_id=1, replica_groups=mesh['kv'=8,'tp'=4] {'tp'}, dimensions={1}, use_global_device_ids=true | all-gather | bytes 81920 | tf_op jit(solution)/shard_map/all_gather | solution.py:213
  7.2 1.8 %copy-done.1 = bf16[512,2816]{1,0:T(8,128)(2,1)S(1)} copy-done((bf16[512,2816]{1,0:T(8,128)(2,1)S(1)}, bf16[512,2816]{1,0:T(8,128)(2,1)}, u32[]{:S(2)}) %copy-start.1) | copy-done | bytes 2883608
  9.0 1.8 %copy-done.2 = bf16[512,2816]{1,0:T(8,128)(2,1)S(1)} copy-done((bf16[512,2816]{1,0:T(8,128)(2,1)S(1)}, bf16[512,2816]{1,0:T(8,128)(2,1)}, u32[]{:S(2)}) %copy-start.2) | copy-done | bytes 2883608
  10.9 0.7 copy-done.11
  11.5 1.1 front.3
  12.7 25.7 %all_to_all.35 = bf16[8,8,5760]{2,1,0:T(8,128)(2,1)S(1)} all-to-all(bf16[8,8,5760]{2,1,0:T(8,128)(2,1)S(1)} %bitcast.39), channel_id=1, replica_groups=mesh['kv'=8,'tp'=4] {'kv'}, dimensions={0} | all-to-all | bytes 1474560 | tf_op jit(solution)/shard_map/all_to_all | solution.py:18
  38.4 0.1 convert_reduce_fusion.1
  38.5 0.2 fusion.35
  38.7 0.1 fusion.8
  38.8 0.0 copy-start.7
  38.8 0.0 copy-start.10
  38.8 0.8 broadcast_in_dim.18
  39.6 4.1 %all-to-all-start.1 = ((bf16[8,8,2816]{2,1,0:T(8,128)(2,1)}), bf16[8,8,2816]{2,1,0:T(8,128)(2,1)}, u32[]{:S(2)}, u32[]{:S(2)}) async-start(bf16[8,8,2816]{2,1,0:T(8,128)(2,1)} %broadcast_in_dim.18), calls=%async_computation.1 | async-start | bytes 720896 | tf_op jit(solution)/shard_map/all_to_all | solution.py:18
  43.7 0.8 copy.36
  44.5 0.1 pad.8.clone
  44.5 1.7 maximum_maximum_fusion.refs_2_
  46.3 8.1 %all-to-all-done.1 = bf16[8,8,2816]{2,1,0:T(8,128)(2,1)} async-done(((bf16[8,8,2816]{2,1,0:T(8,128)(2,1)}), bf16[8,8,2816]{2,1,0:T(8,128)(2,1)}, u32[]{:S(2)}, u32[]{:S(2)}) %all-to-all-start.1) | async-done | bytes 360480 | tf_op jit(solution)/shard_map/all_to_all | solution.py:18
  54.4 1.7 convolution_convert_fusion.1
  56.1 5.8 %all-gather = bf16[256,512]{1,0:T(8,128)(2,1)S(1)} all-gather(bf16[64,512]{1,0:T(8,128)(2,1)S(1)} %convolution_convert_fusion.1), channel_id=2, replica_groups=mesh['kv'=8,'tp'=4] {'tp'}, dimensions={0}, use_global_device_ids=true | all-gather | bytes 327680 | tf_op jit(solution)/shard_map/all_gather | solution.py:23
  62.0 1.0 copy-done.8
  63.1 0.9 copy-done.9
  64.0 0.0 copy-start.17
  64.0 1.9 %front.4 = bf16[64,5248]{1,0:T(8,128)(2,1)} custom-call(bf16[64,512]{1,0:T(8,128)(2,1)S(1)} %add_convert_fusion.1.refs_0_, bf16[512]{0:T(512)(128)(2,1)S(1)} %copy-done.10, bf16[512,128]{1,0:T(8,128)(2,1)S(1)} %copy-done.9, bf16[512,2048]{1,0:T(8,128)(2,1)S(1)} %copy-done.5, bf16[512,2048]{1,0:T(8,128)(2,1)S(1)} %copy-done.6, ...), custom_call_target="tpu_custom_call" | custom-call | flops 343932928 | bytes 5242880 | tf_op jit(solution)/shard_map/front/pallas_call | solution.py:77
  65.9 4.3 %all-to-all-start.2 = ((bf16[8,8,5248]{2,1,0:T(8,128)(2,1)}), bf16[8,8,5248]{2,1,0:T(8,128)(2,1)}, u32[]{:S(2)}, u32[]{:S(2)}) async-start(bf16[8,8,5248]{2,1,0:T(8,128)(2,1)} %bitcast.3), calls=%async_computation.2 | async-start | bytes 1343488 | tf_op jit(solution)/shard_map/all_to_all | solution.py:18
  70.3 0.6 convert_element_type.100
  70.9 1.2 exp.49
  72.1 0.7 mul.284
  72.8 0.7 mul.285
  73.5 1.3 convert_element_type.109
  74.8 13.9 %all-to-all-done.2 = bf16[8,8,5248]{2,1,0:T(8,128)(2,1)} async-done(((bf16[8,8,5248]{2,1,0:T(8,128)(2,1)}), bf16[8,8,5248]{2,1,0:T(8,128)(2,1)}, u32[]{:S(2)}, u32[]{:S(2)}) %all-to-all-start.2) | async-done | bytes 671776 | tf_op jit(solution)/shard_map/all_to_all | solution.py:18
  88.7 1.2 convert_reduce_fusion.2
  89.9 0.2 fusion.29
  90.1 0.1 fusion.20
  90.2 0.7 fusion.15
  91.1 0.8 multiply_reduce_fusion.1
  91.9 0.7 reduce_sum.111
  92.6 0.7 multiply_exponential_fusion
  93.4 1.0 multiply_multiply_fusion
  94.4 9.0 %multiply_reduce_fusion = (f32[8,32,64]{2,1,0:T(8,128)}, f32[8,32,64,128]{3,2,1,0:T(8,128)}) fusion(f32[8,32,128]{2,1,0:T(8,128)S(1)} %broadcast_bitcast_fusion, f32[8,32,128]{2,1,0:T(8,128)S(1)} %broadcast_bitcast_fusion.1, f32[8,32,64]{2,1,0:T(8,128)S(1)} %multiply_multiply_fusion, f32[8,32,64,128]{3,2,1,0:T(8,128)} %param.47, f32[8,32]{1,0:T(8,128)S(1)} %get-tuple-element.9), kind=kLoop, calls=%fused_computation | loop fusion | flops 10469376 | bytes 17171456 | tf_op jit(solution)/shard_map/reduce_sum | solution.py:174
  103.4 1.0 reduce_sum.117
  104.4 0.8 fusion.36
  105.2 0.1 reduce_sum.118
  105.3 0.1 mul.294
  105.3 0.9 multiply_convert_fusion
  106.2 12.6 %all_to_all.36 = bf16[8,8,2048]{2,1,0:T(8,128)(2,1)S(1)} all-to-all(bf16[8,8,2048]{2,1,0:T(8,128)(2,1)S(1)} %broadcast_in_dim.25), channel_id=1, replica_groups=mesh['kv'=8,'tp'=4] {'kv'}, dimensions={0} | all-to-all | bytes 524288 | tf_op jit(solution)/shard_map/all_to_all | solution.py:18
  118.8 2.1 %convolution_convert_fusion.2 = bf16[64,512]{1,0:T(8,128)(2,1)S(1)} fusion(bf16[2048,512]{1,0:T(8,128)(2,1)} %param.49, bf16[8,8,2048]{2,1,0:T(8,128)(2,1)S(1)} %all_to_all.36), kind=kOutput, calls=%fused_computation.7 | convolution fusion | flops 134250496 | bytes 2424832 | tf_op jit(solution)/shard_map/dot_general | solution.py:243
  120.9 5.8 %all-gather.1 = bf16[256,512]{1,0:T(8,128)(2,1)S(1)} all-gather(bf16[64,512]{1,0:T(8,128)(2,1)S(1)} %convolution_convert_fusion.2), channel_id=3, replica_groups=mesh['kv'=8,'tp'=4] {'tp'}, dimensions={0}, use_global_device_ids=true | all-gather | bytes 327680 | tf_op jit(solution)/shard_map/all_gather | solution.py:23
  126.7 1.8 %copy-done.4 = bf16[512,2816]{1,0:T(8,128)(2,1)S(1)} copy-done((bf16[512,2816]{1,0:T(8,128)(2,1)S(1)}, bf16[512,2816]{1,0:T(8,128)(2,1)}, u32[]{:S(2)}) %copy-start.4) | copy-done | bytes 2883608
  128.5 1.1 front.5
  129.7 23.0 %all_to_all.37 = bf16[8,8,5760]{2,1,0:T(8,128)(2,1)S(1)} all-to-all(bf16[8,8,5760]{2,1,0:T(8,128)(2,1)S(1)} %bitcast.40), channel_id=1, replica_groups=mesh['kv'=8,'tp'=4] {'kv'}, dimensions={0} | all-to-all | bytes 1474560 | tf_op jit(solution)/shard_map/all_to_all | solution.py:18
  152.7 0.1 convert_reduce_fusion
  152.8 0.2 fusion.25
  153.0 0.1 fusion.6
  153.1 0.8 broadcast_in_dim.26
  153.8 3.6 %all-to-all-start.5 = ((bf16[8,8,2816]{2,1,0:T(8,128)(2,1)}), bf16[8,8,2816]{2,1,0:T(8,128)(2,1)S(1)}, u32[]{:S(2)}, u32[]{:S(2)}) async-start(bf16[8,8,2816]{2,1,0:T(8,128)(2,1)} %broadcast_in_dim.26), calls=%async_computation.5 | async-start | bytes 720896 | tf_op jit(solution)/shard_map/all_to_all | solution.py:18
  157.4 0.7 fusion.4
  158.1 10.4 %all-to-all-done.5 = bf16[8,8,2816]{2,1,0:T(8,128)(2,1)S(1)} async-done(((bf16[8,8,2816]{2,1,0:T(8,128)(2,1)}), bf16[8,8,2816]{2,1,0:T(8,128)(2,1)S(1)}, u32[]{:S(2)}, u32[]{:S(2)}) %all-to-all-start.5) | async-done | bytes 360480 | tf_op jit(solution)/shard_map/all_to_all | solution.py:18
  168.5 2.4 %fusion = bf16[8,4,8,128]{3,2,1,0:T(8,128)(2,1)S(1)} fusion(bf16[2816,512]{1,0:T(8,128)(2,1)} %param.53, bf16[8,8,2816]{2,1,0:T(8,128)(2,1)S(1)} %all-to-all-done.5), kind=kOutput, calls=%fused_computation.8 | convolution fusion | flops 184582144 | bytes 3309568 | tf_op jit(solution)/shard_map/dot_general | solution.py:133
  170.9 0.6 copy.41
  171.5 3.3 %all-to-all-start.6 = ((bf16[4,64,128]{2,1,0:T(8,128)(2,1)}), bf16[4,64,128]{2,1,0:T(8,128)(2,1)S(1)}, u32[]{:S(2)}, u32[]{:S(2)}) async-start(bf16[4,64,128]{2,1,0:T(8,128)(2,1)} %bitcast.38), calls=%async_computation.6 | async-start | bytes 131072 | tf_op jit(solution)/shard_map/all_to_all | solution.py:18
  174.9 0.6 fusion.16
  175.5 3.4 %all-to-all-done.6 = bf16[4,64,128]{2,1,0:T(8,128)(2,1)S(1)} async-done(((bf16[4,64,128]{2,1,0:T(8,128)(2,1)}), bf16[4,64,128]{2,1,0:T(8,128)(2,1)S(1)}, u32[]{:S(2)}, u32[]{:S(2)}) %all-to-all-start.6) | async-done | bytes 65568 | tf_op jit(solution)/shard_map/all_to_all | solution.py:18
  178.9 0.6 add_convert_fusion.2
  (59 shorter events, 0.4 us)
Async XLA Ops:
  0.6 53.8 %copy-start = (bf16[2816,512]{1,0:T(8,128)(2,1)S(1)}, bf16[2816,512]{1,0:T(8,128)(2,1)}, u32[]{:S(2)}) copy-start(bf16[2816,512]{1,0:T(8,128)(2,1)} %param.31) | copy-start | bytes 8650756
  7.2 1.8 %copy-start.1 = (bf16[512,2816]{1,0:T(8,128)(2,1)S(1)}, bf16[512,2816]{1,0:T(8,128)(2,1)}, u32[]{:S(2)}) copy-start(bf16[512,2816]{1,0:T(8,128)(2,1)} %refs_2_.2) | copy-start | bytes 8650756
  9.0 1.8 %copy-start.2 = (bf16[512,2816]{1,0:T(8,128)(2,1)S(1)}, bf16[512,2816]{1,0:T(8,128)(2,1)}, u32[]{:S(2)}) copy-start(bf16[512,2816]{1,0:T(8,128)(2,1)} %refs_3_.3) | copy-start | bytes 8650756
  10.9 0.7 copy-start.11
  12.7 31.0 %copy-start.21 = (bf16[512,32]{0,1:T(8,128)(2,1)S(1)}, bf16[512,32]{0,1:T(8,128)(2,1)}, u32[]{:S(2)}) copy-start(bf16[512,32]{0,1:T(8,128)(2,1)} %param.37) | copy-start | bytes 98308
  38.8 23.2 %copy-start.7 = (bf16[512,512]{1,0:T(8,128)(2,1)S(1)}, bf16[512,512]{1,0:T(8,128)(2,1)}, u32[]{:S(2)}) copy-start(bf16[512,512]{1,0:T(8,128)(2,1)} %refs_5_.1) | copy-start | bytes 1572868
  38.8 23.2 %copy-start.10 = (bf16[512]{0:T(512)(128)(2,1)S(1)}, bf16[512]{0:T(512)(128)(2,1)}, u32[]{:S(2)}) copy-start(bf16[512]{0:T(512)(128)(2,1)} %refs_1_.4) | copy-start | bytes 3076
  39.6 14.8 %all-to-all-start.1 = ((bf16[8,8,2816]{2,1,0:T(8,128)(2,1)}), bf16[8,8,2816]{2,1,0:T(8,128)(2,1)}, u32[]{:S(2)}, u32[]{:S(2)}) async-start(bf16[8,8,2816]{2,1,0:T(8,128)(2,1)} %broadcast_in_dim.18), calls=%async_computation.1 | async-start | bytes 720896 | tf_op jit(solution)/shard_map/all_to_all | solution.py:18
  54.4 7.6 %copy-start.5 = (bf16[512,2048]{1,0:T(8,128)(2,1)S(1)}, bf16[512,2048]{1,0:T(8,128)(2,1)}, u32[]{:S(2)}) copy-start(bf16[512,2048]{1,0:T(8,128)(2,1)} %refs_3_.4) | copy-start | bytes 6291460
  54.4 7.6 %copy-start.6 = (bf16[512,2048]{1,0:T(8,128)(2,1)S(1)}, bf16[512,2048]{1,0:T(8,128)(2,1)}, u32[]{:S(2)}) copy-start(bf16[512,2048]{1,0:T(8,128)(2,1)} %refs_4_.1) | copy-start | bytes 6291460
  62.0 1.0 copy-start.8
  63.1 0.9 copy-start.9
  64.0 6.3 %copy-start.24 = (bf16[4,512]{1,0:T(4,128)(2,1)S(1)}, bf16[4,512]{1,0:T(4,128)(2,1)}, u32[]{:S(2)}) copy-start(bf16[4,512]{1,0:T(4,128)(2,1)} %param.42) | copy-start | bytes 12292
  64.0 6.3 %copy-start.25 = (bf16[4,512]{1,0:T(4,128)(2,1)S(1)}, bf16[4,512]{1,0:T(4,128)(2,1)}, u32[]{:S(2)}) copy-start(bf16[4,512]{1,0:T(4,128)(2,1)} %param.43) | copy-start | bytes 12292
  64.0 6.3 %copy-start.22 = (bf16[4,2048]{1,0:T(4,128)(2,1)S(1)}, bf16[4,2048]{1,0:T(4,128)(2,1)}, u32[]{:S(2)}) copy-start(bf16[4,2048]{1,0:T(4,128)(2,1)} %param.41) | copy-start | bytes 49156
  64.0 26.9 %copy-start.15 = (bf16[8,3,512]{2,0,1:T(8,128)(2,1)S(1)}, bf16[8,3,512]{2,0,1:T(8,128)(2,1)}, u32[]{:S(2)}) copy-start(bf16[8,3,512]{2,0,1:T(8,128)(2,1)} %param.46) | copy-start | bytes 73732
  64.0 26.9 %copy-start.17 = (bf16[8,3,512]{2,0,1:T(8,128)(2,1)S(1)}, bf16[8,3,512]{2,0,1:T(8,128)(2,1)}, u32[]{:S(2)}) copy-start(bf16[8,3,512]{2,0,1:T(8,128)(2,1)} %param.45) | copy-start | bytes 73732
  65.9 25.1 %copy-start.13 = (bf16[8,3,2048]{2,0,1:T(8,128)(2,1)S(1)}, bf16[8,3,2048]{2,0,1:T(8,128)(2,1)}, u32[]{:S(2)}) copy-start(bf16[8,3,2048]{2,0,1:T(8,128)(2,1)} %param.44) | copy-start | bytes 294916
  65.9 22.8 %all-to-all-start.2 = ((bf16[8,8,5248]{2,1,0:T(8,128)(2,1)}), bf16[8,8,5248]{2,1,0:T(8,128)(2,1)}, u32[]{:S(2)}, u32[]{:S(2)}) async-start(bf16[8,8,5248]{2,1,0:T(8,128)(2,1)} %bitcast.3), calls=%async_computation.2 | async-start | bytes 1343488 | tf_op jit(solution)/shard_map/all_to_all | solution.py:18
  90.1 0.9 copy-start.23
  90.2 0.8 copy-start.19
  103.4 23.4 %copy-start.12 = (bf16[512]{0:T(512)(128)(2,1)S(1)}, bf16[512]{0:T(512)(128)(2,1)}, u32[]{:S(2)}) copy-start(bf16[512]{0:T(512)(128)(2,1)} %refs_1_.5) | copy-start | bytes 3076
  105.3 21.5 %copy-start.3 = (bf16[512,2816]{1,0:T(8,128)(2,1)S(1)}, bf16[512,2816]{1,0:T(8,128)(2,1)}, u32[]{:S(2)}) copy-start(bf16[512,2816]{1,0:T(8,128)(2,1)} %refs_2_.3) | copy-start | bytes 8650756
  126.7 1.8 %copy-start.4 = (bf16[512,2816]{1,0:T(8,128)(2,1)S(1)}, bf16[512,2816]{1,0:T(8,128)(2,1)}, u32[]{:S(2)}) copy-start(bf16[512,2816]{1,0:T(8,128)(2,1)} %refs_3_.5) | copy-start | bytes 8650756
  129.7 27.8 %copy-start.14 = (bf16[8,1,2048]{2,0,1:T(8,128)(2,1)S(1)}, bf16[8,1,2048]{2,0,1:T(8,128)(2,1)}, u32[]{:S(2)}) copy-start(bf16[8,1,2048]{2,0,1:T(8,128)(2,1)} %fusion.15) | copy-start | bytes 98308
  152.7 22.2 %copy-start.16 = (bf16[8,3,512]{2,0,1:T(8,128)(2,1)S(1)}, bf16[8,3,512]{2,0,1:T(8,128)(2,1)}, u32[]{:S(2)}) copy-start(bf16[8,3,512]{2,0,1:T(8,128)(2,1)} %param.46) | copy-start | bytes 73732
  152.7 22.2 %copy-start.18 = (bf16[8,3,512]{2,0,1:T(8,128)(2,1)S(1)}, bf16[8,3,512]{2,0,1:T(8,128)(2,1)}, u32[]{:S(2)}) copy-start(bf16[8,3,512]{2,0,1:T(8,128)(2,1)} %param.45) | copy-start | bytes 73732
  152.7 22.2 %copy-start.20 = (bf16[8,1,512]{2,0,1:T(8,128)(2,1)S(1)}, bf16[8,1,512]{2,0,1:T(8,128)(2,1)}, u32[]{:S(2)}) copy-start(bf16[8,1,512]{2,0,1:T(8,128)(2,1)} %copy-done.19) | copy-start | bytes 24580
  153.8 14.6 %all-to-all-start.5 = ((bf16[8,8,2816]{2,1,0:T(8,128)(2,1)}), bf16[8,8,2816]{2,1,0:T(8,128)(2,1)S(1)}, u32[]{:S(2)}, u32[]{:S(2)}) async-start(bf16[8,8,2816]{2,1,0:T(8,128)(2,1)} %broadcast_in_dim.26), calls=%async_computation.5 | async-start | bytes 720896 | tf_op jit(solution)/shard_map/all_to_all | solution.py:18
  171.5 7.4 %all-to-all-start.6 = ((bf16[4,64,128]{2,1,0:T(8,128)(2,1)}), bf16[4,64,128]{2,1,0:T(8,128)(2,1)S(1)}, u32[]{:S(2)}, u32[]{:S(2)}) async-start(bf16[4,64,128]{2,1,0:T(8,128)(2,1)} %bitcast.38), calls=%async_computation.6 | async-start | bytes 131072 | tf_op jit(solution)/shard_map/all_to_all | solution.py:18
